TPU v7x, 32 devices: a whole 2x2x4 slice. The times are simulated.
32 devices in a mesh: sp: 16 (over z, y, x), tp: 2 (over core).
Axes of the slice: x: 2, y: 2, z: 4, core: 2. Of those that a mesh axis runs over, the one named last changes fastest.
Arguments:
- query_one: bfloat16 [2048, 1024], P('sp', 'tp'), may hold values from -85 to 85
- key_one: bfloat16 [2048, 1024], P('sp', 'tp'), may hold values from -6.5 to 6.5
- query_two: bfloat16 [2048, 1024], P('sp', 'tp'), may hold values from -85 to 85
- key_two: bfloat16 [2048, 1024], P('sp', 'tp'), may hold values from -6.5 to 6.5
- values: bfloat16 [2048, 2048], P('sp', 'tp'), may hold values from -6 to 6
- mix_weight: float32 [8], P('tp'), may hold values from 0.3 to 0.8
- head_gain: float32 [256], replicated, may hold values from 0.1 to 1.9
- residual: bfloat16 [2048, 2048], P(('sp', 'tp')), may hold values from -6 to 6
- out_weight: bfloat16 [2048, 2048], P('tp'), may hold values from -0.125 to 0.125
- norm_gain: float32 [2048], replicated, may hold values from 0.1 to 1.9
- lift_weight: bfloat16 [2048, 5632], P('sp', 'tp'), may hold values from -0.125 to 0.125
- gate_weight: bfloat16 [2048, 5632], P('sp', 'tp'), may hold values from -0.125 to 0.125
- conv_taps: float32 [3, 5632], P(None, 'tp'), may hold values from -3 to 3
- down_weight: bfloat16 [5632, 2048], P('tp'), may hold values from -0.078125 to 0.078125
Outputs:
- layer_out: bfloat16 [2048, 2048], P(('sp', 'tp'))
All inputs are finite; a program needn't handle non-finite values.
Results may differ from a plain program's by a relative error of at most 0.015.
Values may be sent and summed in bfloat16 or wider, within the bound.
A program may use at most 128 MiB of HBM per device.

v0:
```python
import jax
import jax.numpy as jnp
from jax import lax
from jax.sharding import PartitionSpec as P

HD = 128
STRETCH = 64
WIDTH = 3
epsilon = 1e-06
masked_score = -1e30


def passed_along(block, axis, distance):
    devices = range(lax.axis_size(axis))
    route = [(i - distance, i) for i in devices if i - distance in devices]
    return lax.ppermute(block, axis, route)


def update_map(peak, total, acc, queries, keys, vals, visible):
    scores = jnp.einsum("thd,shd->hts", queries, keys, preferred_element_type=jnp.float32) * HD ** (
        -0.5
    )
    scores = jnp.where(visible[None], scores, masked_score)
    new_peak = jnp.maximum(peak, jnp.max(scores, axis=-1))
    weights = jnp.where(visible[None], jnp.exp(scores - new_peak[..., None]), 0.0)
    total = jnp.sum(weights, axis=-1)
    acc = jnp.einsum(
        "hts,she->hte", weights.astype(jnp.bfloat16), vals, preferred_element_type=jnp.float32
    )
    return (new_peak, total, acc)


def on_device(
    query_one,
    key_one,
    query_two,
    key_two,
    values,
    mix_weight,
    head_gain,
    residual,
    out_weight,
    norm_gain,
    lift_weight,
    gate_weight,
    conv_taps,
    down_weight,
):
    tok_local = query_one.shape[0]
    heads_local = mix_weight.shape[0]
    val_width = values.shape[1] // heads_local
    model_width = residual.shape[1]
    offset = lax.axis_index("sp") * tok_local
    q_pos = offset + lax.iota(jnp.int32, tok_local)
    q_one = query_one.reshape(tok_local, heads_local, HD)
    q_two = query_two.reshape(tok_local, heads_local, HD)
    start_peak = jnp.full((heads_local, tok_local), masked_score, jnp.float32)
    start_total = jnp.zeros((heads_local, tok_local), jnp.float32)
    start_acc = jnp.zeros((heads_local, tok_local, val_width), jnp.float32)
    initial = (start_peak, start_total, start_acc, start_peak, start_total, start_acc)
    first_keys = lax.all_gather(key_one, "sp", axis=0, tiled=True)
    second_keys = lax.all_gather(key_two, "sp", axis=0, tiled=True)
    piece_vals = lax.all_gather(values, "sp", axis=0, tiled=True)
    count = first_keys.shape[0]
    k_pos = lax.iota(jnp.int32, count)
    visible = k_pos[None, :] // STRETCH <= q_pos[:, None] // STRETCH
    first_keys = first_keys.reshape(count, heads_local, HD)
    second_keys = second_keys.reshape(count, heads_local, HD)
    piece_vals = piece_vals.reshape(count, heads_local, val_width)
    first = update_map(initial[0], initial[1], initial[2], q_one, first_keys, piece_vals, visible)
    second = update_map(initial[3], initial[4], initial[5], q_two, second_keys, piece_vals, visible)
    state = first + second
    mixed = (
        state[2] / state[1][..., None] - mix_weight[:, None, None] * state[5] / state[4][..., None]
    )
    head_out = (
        mixed * lax.rsqrt(jnp.mean(mixed * mixed, axis=-1, keepdims=True) + epsilon) * head_gain
    ).astype(jnp.bfloat16)
    out_heads = out_weight.reshape(heads_local, val_width, model_width)
    piece = head_out
    attended = lax.psum_scatter(
        jnp.einsum("hte,hed->td", piece, out_heads, preferred_element_type=jnp.float32).astype(
            jnp.bfloat16
        ),
        "tp",
        scatter_dimension=0,
        tiled=True,
    ).astype(jnp.float32)
    stream = residual.astype(jnp.float32) + attended
    normed = (
        stream * lax.rsqrt(jnp.mean(stream * stream, axis=-1, keepdims=True) + epsilon) * norm_gain
    ).astype(jnp.bfloat16)
    whole_rows = lax.all_gather(normed, "tp", axis=0, tiled=True)
    lift_pre = jnp.dot(
        whole_rows,
        lax.all_gather(lift_weight, "sp", axis=0, tiled=True),
        preferred_element_type=jnp.float32,
    )
    gate_pre = jnp.dot(
        whole_rows,
        lax.all_gather(gate_weight, "sp", axis=0, tiled=True),
        preferred_element_type=jnp.float32,
    )
    lifted = lift_pre.astype(jnp.bfloat16)
    gated = gate_pre.astype(jnp.bfloat16)
    prior = passed_along(gated[tok_local - (WIDTH - 1) :], "sp", 1)
    extended = jnp.concatenate([prior, gated], axis=0).astype(jnp.float32)
    conv = conv_taps[0] * extended[0:tok_local]
    for index in range(1, WIDTH):
        conv = conv + conv_taps[index] * extended[index : index + tok_local]
    hidden = (jax.nn.silu(conv) * lifted.astype(jnp.float32)).astype(jnp.bfloat16)
    piece = hidden
    mixer = lax.psum_scatter(
        jnp.dot(piece, down_weight, preferred_element_type=jnp.float32).astype(jnp.bfloat16),
        "tp",
        scatter_dimension=0,
        tiled=True,
    ).astype(jnp.float32)
    return (stream + mixer).astype(jnp.bfloat16)


def solution(mesh):
    return jax.shard_map(
        on_device,
        mesh=mesh,
        in_specs=(
            P("sp", "tp"),
            P("sp", "tp"),
            P("sp", "tp"),
            P("sp", "tp"),
            P("sp", "tp"),
            P("tp"),
            P(),
            P(("sp", "tp"), None),
            P("tp", None),
            P(),
            P("sp", "tp"),
            P("sp", "tp"),
            P(None, "tp"),
            P("tp", None),
        ),
        out_specs=P(("sp", "tp"), None),
        check_vma=False,
    )
```

profile of v0, /device:TPU:0, one launch (start us, length us, event | category | flops | bytes accessed | tf_op | source)
XLA Modules:
  0.0 559.7 jit_solution(8064380941577082344)
XLA Ops:
  6.5 0.0 copy-start
  6.5 0.0 all-gather.6.cloned.1.call-start
  6.5 1.7 copy.17
  8.2 0.0 all-gather.6.cloned.1.call-update
  8.3 0.0 all-gather.10.cloned.1.call-start
  8.3 1.7 copy.22
  10.0 0.0 all-gather.10.cloned.1.call-update
  10.0 0.0 all-gather.8.cloned.1.call-start
  10.0 1.8 copy.20
  11.8 0.0 all-gather.8.cloned.1.call-update
  11.9 0.0 reduce-scatter.3.cloned.1.call-start
  11.9 0.2 broadcast_compare_fusion
  12.2 63.6 %all-gather.6.cloned.1.call-done = bf16[2048,512]{0,1:T(8,128)(2,1)} async-done(((bf16[128,512]{0,1:T(8,128)(2,1)}), bf16[2048,512]{0,1:T(8,128)(2,1)}) %all-gather.6.cloned.1.call-update) | async-done | bytes 2097168 | tf_op jit(solution)/shard_map/all_gather | solution.py:61
  75.7 4.7 fusion
  80.4 59.2 %all-gather.10.cloned.1.call-done = bf16[2048,512]{0,1:T(8,128)(2,1)} async-done(((bf16[128,512]{0,1:T(8,128)(2,1)}), bf16[2048,512]{0,1:T(8,128)(2,1)}) %all-gather.10.cloned.1.call-update) | async-done | bytes 2097168 | tf_op jit(solution)/shard_map/all_gather | solution.py:62
  139.6 5.1 fusion.5
  144.7 0.0 copy-start.3
  144.7 0.0 copy-start.10
  144.7 1.9 copy-done.3
  146.6 1.3 fusion.7
  147.9 81.3 %all-gather.8.cloned.1.call-done = bf16[2048,1024]{0,1:T(8,128)(2,1)} async-done(((bf16[128,1024]{0,1:T(8,128)(2,1)}), bf16[2048,1024]{0,1:T(8,128)(2,1)}) %all-gather.8.cloned.1.call-update) | async-done | bytes 4194320 | tf_op jit(solution)/shard_map/all_gather | solution.py:63
  229.2 5.5 fusion.35
  234.7 0.0 copy-done.2
  234.7 0.4 copy-done.9
  235.2 2.1 multiply_reduce_fusion.1
  237.3 0.0 copy-done.1
  237.4 1.6 fusion.9
  238.9 0.0 reduce-scatter.3.cloned.1.call-update
  239.0 0.0 all-gather.12.cloned.1.call-start
  239.0 0.5 all-gather.12.cloned.1.call-update
  239.6 0.0 all-gather.14.cloned.1.call-start
  239.6 0.5 all-gather.14.cloned.1.call-update
  240.1 0.0 reduce-scatter.5.cloned.1.call-start
  240.2 5.0 reduce-scatter.3.cloned.1.call-done
  245.2 1.1 multiply_reduce_fusion
  246.4 1.1 multiply_convert_fusion
  247.5 2.2 all_gather.21
  249.6 140.8 %all-gather.12.cloned.1.call-done = bf16[2048,2816]{1,0:T(8,128)(2,1)} async-done(((bf16[128,2816]{1,0:T(8,128)(2,1)}), bf16[2048,2816]{1,0:T(8,128)(2,1)}) %all-gather.12.cloned.1.call-update) | async-done | bytes 11534352 | tf_op jit(solution)/shard_map/all_gather | solution.py:101
  390.4 5.9 %convolution_convert_fusion.1 = bf16[128,2816]{1,0:T(8,128)(2,1)S(1)} fusion(bf16[128,2048]{1,0:T(8,128)(2,1)S(1)} %all_gather.21, bf16[2048,2816]{1,0:T(8,128)(2,1)} %all-gather.12.cloned.1.call-done), kind=kOutput, calls=%fused_computation.10 | convolution fusion | flops 1476755456 | bytes 12779520 | tf_op jit(solution)/shard_map/dot_general | solution.py:99
  396.4 3.4 collective-permute-start
  399.8 0.1 slice_reduce_fusion.2
  399.9 1.1 collective-permute-done
  400.9 0.2 maximum_convert_fusion
  401.1 131.5 %all-gather.14.cloned.1.call-done = bf16[2048,2816]{1,0:T(8,128)(2,1)} async-done(((bf16[128,2816]{1,0:T(8,128)(2,1)}), bf16[2048,2816]{1,0:T(8,128)(2,1)}) %all-gather.14.cloned.1.call-update) | async-done | bytes 11534352 | tf_op jit(solution)/shard_map/all_gather | solution.py:96
  532.7 12.1 %convolution_convert_fusion.2 = bf16[128,2048]{1,0:T(8,128)(2,1)} fusion(bf16[2816,2048]{1,0:T(8,128)(2,1)} %param.27, bf16[128,2048]{1,0:T(8,128)(2,1)S(1)} %all_gather.21, bf16[2048,2816]{1,0:T(8,128)(2,1)} %all-gather.14.cloned.1.call-done, f32[130,2816]{1,0:T(8,128)S(1)} %maximum_convert_fusion, f32[2816]{0:T(1024)S(1)} %get-tuple-element.8, ...), kind=kOutput, calls=%fused_computation.17 | convolution fusion | flops 2957737984 | bytes 28479488 | tf_op jit(solution)/shard_map/dot_general | solution.py:114
  544.8 0.0 reduce-scatter.5.cloned.1.call-update
  544.8 6.3 %reduce-scatter.5.cloned.1.call-done = bf16[64,2048]{1,0:T(8,128)(2,1)} async-done(((bf16[128,2048]{1,0:T(8,128)(2,1)}), bf16[64,2048]{1,0:T(8,128)(2,1)}) %reduce-scatter.5.cloned.1.call-update) | async-done | bytes 262160 | tf_op jit(solution)/shard_map/reduce_scatter | solution.py:113
  551.1 1.7 add_convert_fusion
  (22 shorter events, 0.1 us)
Async XLA Ops:
  6.5 133.1 %copy-start = (bf16[128,512]{1,0:T(8,128)(2,1)S(1)}, bf16[128,512]{1,0:T(8,128)(2,1)}, u32[]{:S(2)}) copy-start(bf16[128,512]{1,0:T(8,128)(2,1)} %param.16) | copy-start | bytes 393220
  6.5 69.2 %all-gather.6.cloned.1.call-start = ((), (), s32[]{:S(2)}) async-start(), calls=%async_computation.2 | async-start | bytes 2228224 | tf_op jit(solution)/shard_map/all_gather | solution.py:61
  8.3 131.3 %all-gather.10.cloned.1.call-start = ((), (), s32[]{:S(2)}) async-start(), calls=%async_computation.4 | async-start | bytes 2228224 | tf_op jit(solution)/shard_map/all_gather | solution.py:62
  10.0 219.2 %all-gather.8.cloned.1.call-start = ((), (), s32[]{:S(2)}) async-start(), calls=%async_computation.3 | async-start | bytes 4456448 | tf_op jit(solution)/shard_map/all_gather | solution.py:63
  11.9 233.4 %reduce-scatter.3.cloned.1.call-start = ((), (), s32[]{:S(2)}) async-start(), calls=%async_computation.5 | async-start | bytes 786432 | tf_op jit(solution)/shard_map/reduce_scatter | solution.py:81
  144.7 1.9 copy-start.3
  144.7 84.5 %copy-start.10 = (f32[4]{0:T(128)S(1)}, f32[4]{0:T(128)}, u32[]{:S(2)}) copy-start(f32[4]{0:T(128)} %param.19) | copy-start | bytes 52
  229.2 5.5 copy-start.2
  229.2 5.9 %copy-start.9 = (bf16[2048,1024]{0,1:T(8,128)(2,1)S(1)}, bf16[2048,1024]{0,1:T(8,128)(2,1)}, u32[]{:S(2)}) copy-start(bf16[2048,1024]{0,1:T(8,128)(2,1)} %all-gather.8.cloned.1.call-done) | copy-start | bytes 12582916
  235.2 2.2 copy-start.1
  235.2 2.2 copy-start.8
  237.3 7.9 %copy-start.4 = (bf16[64,2048]{1,0:T(8,128)(2,1)S(1)}, bf16[64,2048]{1,0:T(8,128)(2,1)}, u32[]{:S(2)}) copy-start(bf16[64,2048]{1,0:T(8,128)(2,1)} %param.21) | copy-start | bytes 786436
  237.4 9.0 %copy-start.7 = (f32[2048]{0:T(1024)S(1)}, f32[2048]{0:T(1024)}, u32[]{:S(2)}) copy-start(f32[2048]{0:T(1024)} %param.23) | copy-start | bytes 24580
  239.0 151.4 %all-gather.12.cloned.1.call-start = ((), (), s32[]{:S(2)}) async-start(), calls=%async_computation.6 | async-start | bytes 12255232 | tf_op jit(solution)/shard_map/all_gather | solution.py:101
  239.6 293.1 %all-gather.14.cloned.1.call-start = ((), (), s32[]{:S(2)}) async-start(), calls=%async_computation.7 | async-start | bytes 12255232 | tf_op jit(solution)/shard_map/all_gather | solution.py:96
  240.1 310.9 %reduce-scatter.5.cloned.1.call-start = ((), (), s32[]{:S(2)}) async-start(), calls=%async_computation.8 | async-start | bytes 786432 | tf_op jit(solution)/shard_map/reduce_scatter | solution.py:113
  249.6 150.1 %copy-start.6 = (f32[3,2816]{1,0:T(4,128)S(1)}, f32[3,2816]{1,0:T(4,128)}, u32[]{:S(2)}) copy-start(f32[3,2816]{1,0:T(4,128)} %param.26) | copy-start | bytes 101380
  396.4 4.6 collective-permute-start
  532.7 18.4 %copy-start.5 = (bf16[64,2048]{1,0:T(8,128)(2,1)S(1)}, bf16[64,2048]{1,0:T(8,128)(2,1)}, u32[]{:S(2)}) copy-start(bf16[64,2048]{1,0:T(8,128)(2,1)} %reduce-scatter.3.cloned.1.call-done) | copy-start | bytes 786436
Sparse Core Ops, SparseCore 0:
  10.0 65.6 all-gather.5
  78.4 61.1 all-gather.9
  142.3 86.8 all-gather.7
  239.1 6.0 reduce-scatter.2
  247.8 142.5 all-gather.11
  393.0 139.5 all-gather.13
  544.9 6.0 reduce-scatter.4
where the time goes:
time: 560 us
  waiting for transfers between devices  490 us (88%)
  matrix products  37 us (7%)
  between operations  13.6 us (2%)
  local copies, waits for them, and re-layouts  7.68 us (1%)
  other arithmetic  5.62 us (1%)
    all_gather x1, waiting for transfers between devices, on_device(): lax.all_gather(gate_weight, 'sp', axis=0, tiled=True)  141 us
    all_gather x1, waiting for transfers between devices, on_device(): lax.all_gather(lift_weight, 'sp', axis=0, tiled=True)  132 us
    all_gather x1, waiting for transfers between devices, on_device(): piece_vals = lax.all_gather(values, 'sp', axis=0, tiled=True)  81.3 us
    all_gather x1, waiting for transfers between devices, on_device(): first_keys = lax.all_gather(key_one, 'sp', axis=0, tiled=True)  63.6 us
    all_gather x1, waiting for transfers between devices, on_device(): second_keys = lax.all_gather(key_two, 'sp', axis=0, tiled=True)  59.2 us
    dot_general x1, matrix products, on_device(): jnp.dot(piece, down_weight, preferred_element_type=jnp.float32)  12.1 us
  transfers between devices with their start and end apart: 8, of which 8 were waited for; matrix products, arithmetic and copies ran while one was open for 4% of the time, Pallas kernels for 0%

commit v1 on v0

--- a/solution.py
+++ b/solution.py
@@ -59,7 +59,14 @@
     start_acc = jnp.zeros((heads_local, tok_local, val_width), jnp.float32)
     initial = (start_peak, start_total, start_acc, start_peak, start_total, start_acc)
     first_keys = lax.all_gather(key_one, "sp", axis=0, tiled=True)
-    second_keys = lax.all_gather(key_two, "sp", axis=0, tiled=True)
+    size = lax.axis_size("sp")
+    forward = [(i_2, (i_2 + 1) % size) for i_2 in range(size)]
+    parts = [key_two]
+    for hop in range(1, size):
+        parts = [lax.ppermute(parts[0], "sp", forward), *parts]
+    full = jnp.concatenate(parts, axis=0)
+    offset_2 = (lax.axis_index("sp") + 1) * parts[-1].shape[0]
+    second_keys = jnp.roll(full, offset_2, axis=0)
     piece_vals = lax.all_gather(values, "sp", axis=0, tiled=True)
     count = first_keys.shape[0]
     k_pos = lax.iota(jnp.int32, count)

time: 560 us -> 515 us (0.920)
  waiting for transfers between devices: 490 us -> 446 us
    ppermute x0 -> x15, waiting for transfers between devices: none -> 143 us  [on_device(): parts = [lax.ppermute(parts[0], 'sp', forward), *parts]]
    all_gather x1, waiting for transfers between devices: 81.3 us -> 15.9 us  [on_device(): piece_vals = lax.all_gather(values, 'sp', axis=0, tiled=True)]
    all_gather x1, waiting for transfers between devices: 63.6 us -> 0.02 us  [on_device(): first_keys = lax.all_gather(key_one, 'sp', axis=0, tiled=True)]
    all_gather x1 -> x0, waiting for transfers between devices: 59.2 us -> none  [on_device(): second_keys = lax.all_gather(key_two, 'sp', axis=0, tiled=True)]
  transfers between devices with their start and end apart: 8 -> 22, of which waited for: 8 -> 21; matrix products, arithmetic and copies ran while one was open for 4% -> 4% of each run, Pallas kernels for 0% -> 0%
where the time goes in v1:
time: 515 us
  waiting for transfers between devices  446 us (87%)
  matrix products  32.3 us (6%)
  between operations  14 us (3%)
  local copies, waits for them, and re-layouts  8.53 us (2%)
  starting transfers between devices  6.43 us (1%)
  other arithmetic  5.62 us (1%)
    ppermute x15, waiting for transfers between devices, on_device(): parts = [lax.ppermute(parts[0], 'sp', forward), *parts]  143 us
    all_gather x1, waiting for transfers between devices, on_device(): lax.all_gather(gate_weight, 'sp', axis=0, tiled=True)  141 us
    all_gather x1, waiting for transfers between devices, on_device(): lax.all_gather(lift_weight, 'sp', axis=0, tiled=True)  132 us
    all_gather x1, waiting for transfers between devices, on_device(): piece_vals = lax.all_gather(values, 'sp', axis=0, tiled=True)  15.9 us
    dot_general x1, matrix products, on_device(): jnp.dot(piece, down_weight, preferred_element_type=jnp.float32)  12.2 us
  transfers between devices with their start and end apart: 22, of which 21 were waited for; matrix products, arithmetic and copies ran while one was open for 4% of the time, Pallas kernels for 0%

profile of v1, /device:TPU:0, one launch (start us, length us, event | category | flops | bytes accessed | tf_op | source)
XLA Modules:
  0.0 514.7 jit_solution(15980985146507221859)
XLA Ops:
  6.5 1.7 copy.18
  8.3 0.0 all-gather.7.cloned.1.call-start
  8.3 1.0 copy.23
  9.3 3.0 collective-permute-start
  12.4 7.5 %collective-permute-done = bf16[128,512]{0,1:T(8,128)(2,1)S(1)} collective-permute-done((bf16[128,512]{0,1:T(8,128)(2,1)S(1)}, bf16[128,512]{0,1:T(8,128)(2,1)S(1)}, u32[]{:S(2)}, u32[]{:S(2)}) %collective-permute-start) | collective-permute-done | bytes 131104 | tf_op jit(solution)/shard_map/ppermute | solution.py:66
  19.9 8.6 %collective-permute-done.1 = bf16[128,512]{0,1:T(8,128)(2,1)S(1)} collective-permute-done((bf16[128,512]{0,1:T(8,128)(2,1)S(1)}, bf16[128,512]{0,1:T(8,128)(2,1)S(1)}, u32[]{:S(2)}, u32[]{:S(2)}) %collective-permute-start.1) | collective-permute-done | bytes 131104 | tf_op jit(solution)/shard_map/ppermute | solution.py:66
  28.4 8.6 %collective-permute-done.2 = bf16[128,512]{0,1:T(8,128)(2,1)S(1)} collective-permute-done((bf16[128,512]{0,1:T(8,128)(2,1)S(1)}, bf16[128,512]{0,1:T(8,128)(2,1)S(1)}, u32[]{:S(2)}, u32[]{:S(2)}) %collective-permute-start.2) | collective-permute-done | bytes 131104 | tf_op jit(solution)/shard_map/ppermute | solution.py:66
  37.0 1.8 copy.21
  38.9 7.1 %collective-permute-done.3 = bf16[128,512]{0,1:T(8,128)(2,1)S(1)} collective-permute-done((bf16[128,512]{0,1:T(8,128)(2,1)S(1)}, bf16[128,512]{0,1:T(8,128)(2,1)S(1)}, u32[]{:S(2)}, u32[]{:S(2)}) %collective-permute-start.3) | collective-permute-done | bytes 131104 | tf_op jit(solution)/shard_map/ppermute | solution.py:66
  45.9 8.7 %collective-permute-done.4 = bf16[128,512]{0,1:T(8,128)(2,1)S(1)} collective-permute-done((bf16[128,512]{0,1:T(8,128)(2,1)S(1)}, bf16[128,512]{0,1:T(8,128)(2,1)S(1)}, u32[]{:S(2)}, u32[]{:S(2)}) %collective-permute-start.4) | collective-permute-done | bytes 131104 | tf_op jit(solution)/shard_map/ppermute | solution.py:66
  54.7 9.1 %collective-permute-done.5 = bf16[128,512]{0,1:T(8,128)(2,1)S(1)} collective-permute-done((bf16[128,512]{0,1:T(8,128)(2,1)S(1)}, bf16[128,512]{0,1:T(8,128)(2,1)S(1)}, u32[]{:S(2)}, u32[]{:S(2)}) %collective-permute-start.5) | collective-permute-done | bytes 131104 | tf_op jit(solution)/shard_map/ppermute | solution.py:66
  63.8 10.8 %collective-permute-done.6 = bf16[128,512]{0,1:T(8,128)(2,1)S(1)} collective-permute-done((bf16[128,512]{0,1:T(8,128)(2,1)S(1)}, bf16[128,512]{0,1:T(8,128)(2,1)S(1)}, u32[]{:S(2)}, u32[]{:S(2)}) %collective-permute-start.6) | collective-permute-done | bytes 131104 | tf_op jit(solution)/shard_map/ppermute | solution.py:66
  74.6 11.6 %collective-permute-done.7 = bf16[128,512]{0,1:T(8,128)(2,1)S(1)} collective-permute-done((bf16[128,512]{0,1:T(8,128)(2,1)S(1)}, bf16[128,512]{0,1:T(8,128)(2,1)S(1)}, u32[]{:S(2)}, u32[]{:S(2)}) %collective-permute-start.7) | collective-permute-done | bytes 131104 | tf_op jit(solution)/shard_map/ppermute | solution.py:66
  86.2 8.6 %collective-permute-done.8 = bf16[128,512]{0,1:T(8,128)(2,1)S(1)} collective-permute-done((bf16[128,512]{0,1:T(8,128)(2,1)S(1)}, bf16[128,512]{0,1:T(8,128)(2,1)S(1)}, u32[]{:S(2)}, u32[]{:S(2)}) %collective-permute-start.8) | collective-permute-done | bytes 131104 | tf_op jit(solution)/shard_map/ppermute | solution.py:66
  94.8 9.8 %collective-permute-done.9 = bf16[128,512]{0,1:T(8,128)(2,1)S(1)} collective-permute-done((bf16[128,512]{0,1:T(8,128)(2,1)S(1)}, bf16[128,512]{0,1:T(8,128)(2,1)S(1)}, u32[]{:S(2)}, u32[]{:S(2)}) %collective-permute-start.9) | collective-permute-done | bytes 131104 | tf_op jit(solution)/shard_map/ppermute | solution.py:66
  104.6 9.1 %collective-permute-done.10 = bf16[128,512]{0,1:T(8,128)(2,1)S(1)} collective-permute-done((bf16[128,512]{0,1:T(8,128)(2,1)S(1)}, bf16[128,512]{0,1:T(8,128)(2,1)S(1)}, u32[]{:S(2)}, u32[]{:S(2)}) %collective-permute-start.10) | collective-permute-done | bytes 131104 | tf_op jit(solution)/shard_map/ppermute | solution.py:66
  113.6 12.2 %collective-permute-done.11 = bf16[128,512]{0,1:T(8,128)(2,1)S(1)} collective-permute-done((bf16[128,512]{0,1:T(8,128)(2,1)S(1)}, bf16[128,512]{0,1:T(8,128)(2,1)S(1)}, u32[]{:S(2)}, u32[]{:S(2)}) %collective-permute-start.11) | collective-permute-done | bytes 131104 | tf_op jit(solution)/shard_map/ppermute | solution.py:66
  125.8 11.9 %collective-permute-done.12 = bf16[128,512]{0,1:T(8,128)(2,1)S(1)} collective-permute-done((bf16[128,512]{0,1:T(8,128)(2,1)S(1)}, bf16[128,512]{0,1:T(8,128)(2,1)S(1)}, u32[]{:S(2)}, u32[]{:S(2)}) %collective-permute-start.12) | collective-permute-done | bytes 131104 | tf_op jit(solution)/shard_map/ppermute | solution.py:66
  137.7 8.5 %collective-permute-done.13 = bf16[128,512]{0,1:T(8,128)(2,1)S(1)} collective-permute-done((bf16[128,512]{0,1:T(8,128)(2,1)S(1)}, bf16[128,512]{0,1:T(8,128)(2,1)S(1)}, u32[]{:S(2)}, u32[]{:S(2)}) %collective-permute-start.13) | collective-permute-done | bytes 131104 | tf_op jit(solution)/shard_map/ppermute | solution.py:66
  146.3 0.2 broadcast_compare_fusion
  146.5 11.3 %collective-permute-done.14 = bf16[128,512]{0,1:T(8,128)(2,1)S(1)} collective-permute-done((bf16[128,512]{0,1:T(8,128)(2,1)S(1)}, bf16[128,512]{0,1:T(8,128)(2,1)S(1)}, u32[]{:S(2)}, u32[]{:S(2)}) %collective-permute-start.14) | collective-permute-done | bytes 131104 | tf_op jit(solution)/shard_map/ppermute | solution.py:66
  159.3 0.1 constant_dynamic-slice_fusion
  159.4 2.8 fusion
  162.2 2.3 fusion.5
  164.6 1.9 copy-done.5
  166.5 1.3 fusion.7
  167.8 15.9 %all-gather.7.cloned.1.call-done = bf16[2048,1024]{0,1:T(8,128)(2,1)} async-done(((bf16[128,1024]{0,1:T(8,128)(2,1)}), bf16[2048,1024]{0,1:T(8,128)(2,1)}) %all-gather.7.cloned.1.call-update) | async-done | bytes 4194320 | tf_op jit(solution)/shard_map/all_gather | solution.py:70
  183.7 5.5 %fusion.35 = f32[4,128,256]{2,1,0:T(8,128)S(1)} fusion(bf16[2048,4,256]{0,2,1:T(8,128)(2,1)} %bitcast.54, f32[4,2048,128]{1,2,0:T(8,128)} %copy-done.5, f32[4,128]{1,0:T(4,128)S(1)} %broadcast_maximum_fusion, pred[128,2048]{1,0:T(8,128)(4,1)S(1)} %broadcast_compare_fusion, f32[4,128]{1,0:T(4,128)S(1)} %fusion.7, f32[4]{0:T(128)S(1)} %copy-done.13), kind=kOutput, calls=%fused_computation.38 | convolution fusion | flops 542375936 | bytes 9179152 | tf_op jit(solution)/shard_map/hts,she->hte/dot_general | solution.py:27
  189.2 0.4 copy-done.12
  189.6 2.1 multiply_reduce_fusion.1
  191.7 0.1 copy-done.2
  191.8 1.6 fusion.9
  193.5 0.5 all-gather.9.cloned.1.call-update
  194.1 0.5 all-gather.11.cloned.1.call-update
  194.6 5.6 %reduce-scatter.3.cloned.1.call-done = bf16[64,2048]{1,0:T(8,128)(2,1)} async-done(((bf16[128,2048]{1,0:T(8,128)(2,1)}), bf16[64,2048]{1,0:T(8,128)(2,1)}) %reduce-scatter.3.cloned.1.call-update) | async-done | bytes 262160 | tf_op jit(solution)/shard_map/reduce_scatter | solution.py:88
  200.3 1.1 multiply_reduce_fusion
  201.4 1.1 multiply_convert_fusion
  202.5 2.4 all_gather.17
  204.9 140.6 %all-gather.9.cloned.1.call-done = bf16[2048,2816]{1,0:T(8,128)(2,1)} async-done(((bf16[128,2816]{1,0:T(8,128)(2,1)}), bf16[2048,2816]{1,0:T(8,128)(2,1)}) %all-gather.9.cloned.1.call-update) | async-done | bytes 11534352 | tf_op jit(solution)/shard_map/all_gather | solution.py:108
  345.5 6.0 %convolution_convert_fusion.1 = bf16[128,2816]{1,0:T(8,128)(2,1)S(1)} fusion(bf16[128,2048]{1,0:T(8,128)(2,1)S(1)} %all_gather.17, bf16[2048,2816]{1,0:T(8,128)(2,1)} %all-gather.9.cloned.1.call-done), kind=kOutput, calls=%fused_computation.10 | convolution fusion | flops 1476755456 | bytes 12779520 | tf_op jit(solution)/shard_map/dot_general | solution.py:106
  351.4 3.2 collective-permute-start.15
  354.6 0.1 slice_reduce_fusion.2
  354.7 1.3 collective-permute-done.15
  356.0 0.2 maximum_convert_fusion
  356.2 131.5 %all-gather.11.cloned.1.call-done = bf16[2048,2816]{1,0:T(8,128)(2,1)} async-done(((bf16[128,2816]{1,0:T(8,128)(2,1)}), bf16[2048,2816]{1,0:T(8,128)(2,1)}) %all-gather.11.cloned.1.call-update) | async-done | bytes 11534352 | tf_op jit(solution)/shard_map/all_gather | solution.py:103
  487.7 12.2 %convolution_convert_fusion.2 = bf16[128,2048]{1,0:T(8,128)(2,1)} fusion(bf16[2816,2048]{1,0:T(8,128)(2,1)} %param.27, bf16[128,2048]{1,0:T(8,128)(2,1)S(1)} %all_gather.17, bf16[2048,2816]{1,0:T(8,128)(2,1)} %all-gather.11.cloned.1.call-done, f32[130,2816]{1,0:T(8,128)S(1)} %maximum_convert_fusion, f32[2816]{0:T(1024)S(1)} %get-tuple-element.8, ...), kind=kOutput, calls=%fused_computation.17 | convolution fusion | flops 2957737984 | bytes 28479488 | tf_op jit(solution)/shard_map/dot_general | solution.py:121
  499.9 6.3 %reduce-scatter.5.cloned.1.call-done = bf16[64,2048]{1,0:T(8,128)(2,1)} async-done(((bf16[128,2048]{1,0:T(8,128)(2,1)}), bf16[64,2048]{1,0:T(8,128)(2,1)}) %reduce-scatter.5.cloned.1.call-update) | async-done | bytes 262160 | tf_op jit(solution)/shard_map/reduce_scatter | solution.py:120
  506.1 1.7 add_convert_fusion
  (88 shorter events, 1.6 us)
Async XLA Ops:
  6.5 155.7 %copy-start = (bf16[128,512]{1,0:T(8,128)(2,1)S(1)}, bf16[128,512]{1,0:T(8,128)(2,1)}, u32[]{:S(2)}) copy-start(bf16[128,512]{1,0:T(8,128)(2,1)} %param.16) | copy-start | bytes 393220
  6.5 152.9 %all-gather.5.cloned.1.call-start = ((), (), s32[]{:S(2)}) async-start(), calls=%async_computation.2 | async-start | bytes 2228224 | tf_op jit(solution)/shard_map/all_gather | solution.py:61
  8.3 175.4 %all-gather.7.cloned.1.call-start = ((), (), s32[]{:S(2)}) async-start(), calls=%async_computation.3 | async-start | bytes 4456448 | tf_op jit(solution)/shard_map/all_gather | solution.py:70
  9.3 10.5 %collective-permute-start = (bf16[128,512]{0,1:T(8,128)(2,1)S(1)}, bf16[128,512]{0,1:T(8,128)(2,1)S(1)}, u32[]{:S(2)}, u32[]{:S(2)}) collective-permute-start(bf16[128,512]{0,1:T(8,128)(2,1)S(1)} %copy.23), channel_id=1, source_target_pairs={{0,2},{2,4},{4,6},{6,8},{8,10},{10,12},{12,14},{14,16},{16,18},{18... | collective-permute-start | bytes 393224 | tf_op jit(solution)/shard_map/ppermute | solution.py:66
  19.8 8.6 %collective-permute-start.1 = (bf16[128,512]{0,1:T(8,128)(2,1)S(1)}, bf16[128,512]{0,1:T(8,128)(2,1)S(1)}, u32[]{:S(2)}, u32[]{:S(2)}) collective-permute-start(bf16[128,512]{0,1:T(8,128)(2,1)S(1)} %collective-permute-done), channel_id=1, source_target_pairs={{0,2},{2,4},{4,6},{6,8},{8,10},{10,12},{12,14},{14,16},{16,18},{18... | collective-permute-start | bytes 393224 | tf_op jit(solution)/shard_map/ppermute | solution.py:66
  28.4 8.6 %collective-permute-start.2 = (bf16[128,512]{0,1:T(8,128)(2,1)S(1)}, bf16[128,512]{0,1:T(8,128)(2,1)S(1)}, u32[]{:S(2)}, u32[]{:S(2)}) collective-permute-start(bf16[128,512]{0,1:T(8,128)(2,1)S(1)} %collective-permute-done.1), channel_id=1, source_target_pairs={{0,2},{2,4},{4,6},{6,8},{8,10},{10,12},{12,14},{14,16},{16,18},{18... | collective-permute-start | bytes 393224 | tf_op jit(solution)/shard_map/ppermute | solution.py:66
  37.0 8.9 %collective-permute-start.3 = (bf16[128,512]{0,1:T(8,128)(2,1)S(1)}, bf16[128,512]{0,1:T(8,128)(2,1)S(1)}, u32[]{:S(2)}, u32[]{:S(2)}) collective-permute-start(bf16[128,512]{0,1:T(8,128)(2,1)S(1)} %collective-permute-done.2), channel_id=1, source_target_pairs={{0,2},{2,4},{4,6},{6,8},{8,10},{10,12},{12,14},{14,16},{16,18},{18... | collective-permute-start | bytes 393224 | tf_op jit(solution)/shard_map/ppermute | solution.py:66
  38.8 161.5 %reduce-scatter.3.cloned.1.call-start = ((), (), s32[]{:S(2)}) async-start(), calls=%async_computation.4 | async-start | bytes 786432 | tf_op jit(solution)/shard_map/reduce_scatter | solution.py:88
  45.9 8.7 %collective-permute-start.4 = (bf16[128,512]{0,1:T(8,128)(2,1)S(1)}, bf16[128,512]{0,1:T(8,128)(2,1)S(1)}, u32[]{:S(2)}, u32[]{:S(2)}) collective-permute-start(bf16[128,512]{0,1:T(8,128)(2,1)S(1)} %collective-permute-done.3), channel_id=1, source_target_pairs={{0,2},{2,4},{4,6},{6,8},{8,10},{10,12},{12,14},{14,16},{16,18},{18... | collective-permute-start | bytes 393224 | tf_op jit(solution)/shard_map/ppermute | solution.py:66
  54.7 9.1 %collective-permute-start.5 = (bf16[128,512]{0,1:T(8,128)(2,1)S(1)}, bf16[128,512]{0,1:T(8,128)(2,1)S(1)}, u32[]{:S(2)}, u32[]{:S(2)}) collective-permute-start(bf16[128,512]{0,1:T(8,128)(2,1)S(1)} %collective-permute-done.4), channel_id=1, source_target_pairs={{0,2},{2,4},{4,6},{6,8},{8,10},{10,12},{12,14},{14,16},{16,18},{18... | collective-permute-start | bytes 393224 | tf_op jit(solution)/shard_map/ppermute | solution.py:66
  63.8 10.9 %collective-permute-start.6 = (bf16[128,512]{0,1:T(8,128)(2,1)S(1)}, bf16[128,512]{0,1:T(8,128)(2,1)S(1)}, u32[]{:S(2)}, u32[]{:S(2)}) collective-permute-start(bf16[128,512]{0,1:T(8,128)(2,1)S(1)} %collective-permute-done.5), channel_id=1, source_target_pairs={{0,2},{2,4},{4,6},{6,8},{8,10},{10,12},{12,14},{14,16},{16,18},{18... | collective-permute-start | bytes 393224 | tf_op jit(solution)/shard_map/ppermute | solution.py:66
  74.6 11.6 %collective-permute-start.7 = (bf16[128,512]{0,1:T(8,128)(2,1)S(1)}, bf16[128,512]{0,1:T(8,128)(2,1)S(1)}, u32[]{:S(2)}, u32[]{:S(2)}) collective-permute-start(bf16[128,512]{0,1:T(8,128)(2,1)S(1)} %collective-permute-done.6), channel_id=1, source_target_pairs={{0,2},{2,4},{4,6},{6,8},{8,10},{10,12},{12,14},{14,16},{16,18},{18... | collective-permute-start | bytes 393224 | tf_op jit(solution)/shard_map/ppermute | solution.py:66
  86.2 8.6 %collective-permute-start.8 = (bf16[128,512]{0,1:T(8,128)(2,1)S(1)}, bf16[128,512]{0,1:T(8,128)(2,1)S(1)}, u32[]{:S(2)}, u32[]{:S(2)}) collective-permute-start(bf16[128,512]{0,1:T(8,128)(2,1)S(1)} %collective-permute-done.7), channel_id=1, source_target_pairs={{0,2},{2,4},{4,6},{6,8},{8,10},{10,12},{12,14},{14,16},{16,18},{18... | collective-permute-start | bytes 393224 | tf_op jit(solution)/shard_map/ppermute | solution.py:66
  94.8 9.8 %collective-permute-start.9 = (bf16[128,512]{0,1:T(8,128)(2,1)S(1)}, bf16[128,512]{0,1:T(8,128)(2,1)S(1)}, u32[]{:S(2)}, u32[]{:S(2)}) collective-permute-start(bf16[128,512]{0,1:T(8,128)(2,1)S(1)} %collective-permute-done.8), channel_id=1, source_target_pairs={{0,2},{2,4},{4,6},{6,8},{8,10},{10,12},{12,14},{14,16},{16,18},{18... | collective-permute-start | bytes 393224 | tf_op jit(solution)/shard_map/ppermute | solution.py:66
  104.6 9.1 %collective-permute-start.10 = (bf16[128,512]{0,1:T(8,128)(2,1)S(1)}, bf16[128,512]{0,1:T(8,128)(2,1)S(1)}, u32[]{:S(2)}, u32[]{:S(2)}) collective-permute-start(bf16[128,512]{0,1:T(8,128)(2,1)S(1)} %collective-permute-done.9), channel_id=1, source_target_pairs={{0,2},{2,4},{4,6},{6,8},{8,10},{10,12},{12,14},{14,16},{16,18},{18... | collective-permute-start | bytes 393224 | tf_op jit(solution)/shard_map/ppermute | solution.py:66
  113.6 12.2 %collective-permute-start.11 = (bf16[128,512]{0,1:T(8,128)(2,1)S(1)}, bf16[128,512]{0,1:T(8,128)(2,1)S(1)}, u32[]{:S(2)}, u32[]{:S(2)}) collective-permute-start(bf16[128,512]{0,1:T(8,128)(2,1)S(1)} %collective-permute-done.10), channel_id=1, source_target_pairs={{0,2},{2,4},{4,6},{6,8},{8,10},{10,12},{12,14},{14,16},{16,18},{18... | collective-permute-start | bytes 393224 | tf_op jit(solution)/shard_map/ppermute | solution.py:66
  125.8 11.9 %collective-permute-start.12 = (bf16[128,512]{0,1:T(8,128)(2,1)S(1)}, bf16[128,512]{0,1:T(8,128)(2,1)S(1)}, u32[]{:S(2)}, u32[]{:S(2)}) collective-permute-start(bf16[128,512]{0,1:T(8,128)(2,1)S(1)} %collective-permute-done.11), channel_id=1, source_target_pairs={{0,2},{2,4},{4,6},{6,8},{8,10},{10,12},{12,14},{14,16},{16,18},{18... | collective-permute-start | bytes 393224 | tf_op jit(solution)/shard_map/ppermute | solution.py:66
  137.7 8.6 %collective-permute-start.13 = (bf16[128,512]{0,1:T(8,128)(2,1)S(1)}, bf16[128,512]{0,1:T(8,128)(2,1)S(1)}, u32[]{:S(2)}, u32[]{:S(2)}) collective-permute-start(bf16[128,512]{0,1:T(8,128)(2,1)S(1)} %collective-permute-done.12), channel_id=1, source_target_pairs={{0,2},{2,4},{4,6},{6,8},{8,10},{10,12},{12,14},{14,16},{16,18},{18... | collective-permute-start | bytes 393224 | tf_op jit(solution)/shard_map/ppermute | solution.py:66
  146.2 11.5 %collective-permute-start.14 = (bf16[128,512]{0,1:T(8,128)(2,1)S(1)}, bf16[128,512]{0,1:T(8,128)(2,1)S(1)}, u32[]{:S(2)}, u32[]{:S(2)}) collective-permute-start(bf16[128,512]{0,1:T(8,128)(2,1)S(1)} %collective-permute-done.13), channel_id=1, source_target_pairs={{0,2},{2,4},{4,6},{6,8},{8,10},{10,12},{12,14},{14,16},{16,18},{18... | collective-permute-start | bytes 393224 | tf_op jit(solution)/shard_map/ppermute | solution.py:66
  158.5 0.9 copy-start.8
  162.2 2.3 copy-start.3
  164.5 2.0 copy-start.5
  164.6 19.2 %copy-start.13 = (f32[4]{0:T(128)S(1)}, f32[4]{0:T(128)}, u32[]{:S(2)}) copy-start(f32[4]{0:T(128)} %param.19) | copy-start | bytes 52
  183.7 5.5 %copy-start.4 = (f32[4,128,2048]{2,1,0:T(8,128)S(1)}, f32[4,128,2048]{2,1,0:T(8,128)}, u32[]{:S(2)}) copy-start(f32[4,128,2048]{2,1,0:T(8,128)} %copy-done.3) | copy-start | bytes 12582916
  183.7 5.9 %copy-start.12 = (bf16[2048,1024]{0,1:T(8,128)(2,1)S(1)}, bf16[2048,1024]{0,1:T(8,128)(2,1)}, u32[]{:S(2)}) copy-start(bf16[2048,1024]{0,1:T(8,128)(2,1)} %all-gather.7.cloned.1.call-done) | copy-start | bytes 12582916
  189.6 2.2 copy-start.2
  189.6 2.2 copy-start.11
  191.8 8.5 %copy-start.6 = (bf16[64,2048]{1,0:T(8,128)(2,1)S(1)}, bf16[64,2048]{1,0:T(8,128)(2,1)}, u32[]{:S(2)}) copy-start(bf16[64,2048]{1,0:T(8,128)(2,1)} %param.21) | copy-start | bytes 786436
  191.8 9.6 %copy-start.10 = (f32[2048]{0:T(1024)S(1)}, f32[2048]{0:T(1024)}, u32[]{:S(2)}) copy-start(f32[2048]{0:T(1024)} %param.23) | copy-start | bytes 24580
  193.4 152.0 %all-gather.9.cloned.1.call-start = ((), (), s32[]{:S(2)}) async-start(), calls=%async_computation.5 | async-start | bytes 12255232 | tf_op jit(solution)/shard_map/all_gather | solution.py:108
  194.0 293.7 %all-gather.11.cloned.1.call-start = ((), (), s32[]{:S(2)}) async-start(), calls=%async_computation.6 | async-start | bytes 12255232 | tf_op jit(solution)/shard_map/all_gather | solution.py:103
  194.6 311.5 %reduce-scatter.5.cloned.1.call-start = ((), (), s32[]{:S(2)}) async-start(), calls=%async_computation.7 | async-start | bytes 786432 | tf_op jit(solution)/shard_map/reduce_scatter | solution.py:120
  204.9 149.7 %copy-start.9 = (f32[3,2816]{1,0:T(4,128)S(1)}, f32[3,2816]{1,0:T(4,128)}, u32[]{:S(2)}) copy-start(f32[3,2816]{1,0:T(4,128)} %param.26) | copy-start | bytes 101380
  351.4 4.6 collective-permute-start.15
  487.7 18.4 %copy-start.7 = (bf16[64,2048]{1,0:T(8,128)(2,1)S(1)}, bf16[64,2048]{1,0:T(8,128)(2,1)}, u32[]{:S(2)}) copy-start(bf16[64,2048]{1,0:T(8,128)(2,1)} %reduce-scatter.3.cloned.1.call-done) | copy-start | bytes 786436
  487.7 20.2 %copy-start.1 = (bf16[128,512]{1,0:T(8,128)(2,1)S(1)}, bf16[128,512]{1,0:T(8,128)(2,1)}, u32[]{:S(2)}) copy-start(bf16[128,512]{1,0:T(8,128)(2,1)} %param.16) | copy-start | bytes 393220
Sparse Core Ops, SparseCore 0:
  10.0 73.1 all-gather.4
  86.0 97.6 all-gather.6
  193.5 6.6 reduce-scatter.2
  202.9 142.5 all-gather.8
  348.1 139.5 all-gather.10
  500.0 6.0 reduce-scatter.4
